TPU v7x, 32 devices: a whole 2x2x4 slice. The times are simulated.
32 devices in a mesh: grp: 2 (over y), ep: 4 (over z), tp: 4 (over x, core).
Axes of the slice: x: 2, y: 2, z: 4, core: 2. Of those that a mesh axis runs over, the one named last changes fastest.
Arguments:
- tokens: bfloat16 [2048, 2048], P(('grp', 'ep', 'tp')), parts along dimension 0, may hold values from -6 to 6
- gain_in: float32 [2048], replicated, may hold values from 0.1 to 1.9
- routes: int32 [2048, 2], P(('grp', 'ep')), parts along dimension 0, may hold values from 0 to 3, all different within a row; in each aligned block of 64 rows (0 to 63, 64 to 127, ...) at most 48 rows name the same one
- gates: float32 [2048, 2], P(('grp', 'ep')), parts along dimension 0, may hold values from 0.05 to 1
- w_gate: bfloat16 [4, 2048, 3072], P('ep', None, 'tp'), may hold values from -0.125 to 0.125
- w_up: bfloat16 [4, 2048, 3072], P('ep', None, 'tp'), may hold values from -0.125 to 0.125
- w_down: bfloat16 [4, 3072, 2048], P('ep', 'tp'), may hold values from -0.109375 to 0.109375
- gain_out: float32 [2048], P('tp'), may hold values from 0.3 to 3
Outputs:
- mixed: bfloat16 [2048, 2048], P(('grp', 'ep'), 'tp'), parts along dimension 0
There are 2 independent parts, one for each index of `grp`. A program takes and returns all parts, laid end to end along the dimension named above; an argument that names none is the same for every part. Nothing has to cross between parts.
Inputs may be any that keep to these rules, and one draw needn't show every extreme that they name: `routes`: each row names 2 different experts; every expert is named by some row. Among the rows of one device (aligned blocks of 64 rows) no expert is named more than 48 times, and in every draw some expert is named exactly 48 times in some such block.
All inputs are finite; a program needn't handle non-finite values.
Results may differ from a plain program's by a relative error of at most 0.012.
Values may be sent and summed in bfloat16 or wider, within the bound.
A program may use at most 64 MiB of HBM per device.

v0:
```python
import functools

import jax
import jax.numpy as jnp
from jax import lax
from jax.experimental import pallas as pl
from jax.experimental.pallas import tpu as pltpu
from jax.sharding import PartitionSpec as P

EPS = 1e-06


def slot_table(routes, experts, capacity):
    sources, count, choose = routes.shape
    flat = routes.reshape(sources, count * choose)
    onehot = (flat[:, :, None] == jnp.arange(experts, dtype=jnp.int32)[None, None, :]).astype(
        jnp.int32
    )
    earlier = jnp.cumsum(onehot, axis=1) - onehot
    slot = jnp.sum(earlier * onehot, axis=2)
    return (flat * capacity + slot).reshape(sources, count, choose)


MESH = pl.DeviceIdType.MESH


def fused_kernel(
    experts,
    groups,
    capacity,
    tokens_hbm,
    gain_in_hbm,
    routes_hbm,
    gates_hbm,
    w_gate_hbm,
    w_up_hbm,
    w_down_hbm,
    gain_out_hbm,
    out_ref,
    tokens_ref,
    gain_in_ref,
    routes_ref,
    gates_ref,
    gain_out_ref,
    stage,
    table,
    w_gate,
    w_up,
    w_down,
    earlier_ref,
    picked,
    rows,
    hidden,
    part,
    pair_in,
    cross_out,
    cross_in,
    home_out,
    home,
    combined,
    squares,
    weight_sem,
    small_sem,
    d1_send,
    d1_recv,
    d2p_send,
    d2p_recv,
    d2x_send,
    d2x_recv,
    d3_send,
    d3_recv,
    r1_send,
    r1_recv,
    r2_send,
    r2_recv,
    r3_send,
    r3_recv,
    sq_send,
    sq_recv,
):
    z = lax.axis_index("ep")
    q = lax.axis_index("tp")
    core = lax.rem(q, 2)
    plane = q // 2
    partner = q + 1 - 2 * core
    across = lax.rem(q + 2, groups)
    count, width = tokens_ref.shape
    total = out_ref.shape[0]
    choose = routes_ref.shape[0]
    hidden_width = w_gate.shape[1]
    slice_width = out_ref.shape[1]
    block_rows = groups * capacity
    half_width = width // 2
    half_rows = block_rows // 2

    last = experts - 1
    side = z // 2
    inward = z + side * (last - 2 * z)
    near = [inward, 2 - 2 * inward, 1 + 2 * inward, last - inward]
    peer = [p + side * (last - 2 * p) for p in near]
    is_end = inward == 0

    small = [
        pltpu.make_async_copy(src, dst, small_sem.at[i])
        for i, (src, dst) in enumerate(
            (
                (tokens_hbm, tokens_ref),
                (routes_hbm, routes_ref),
                (gates_hbm, gates_ref),
                (gain_in_hbm, gain_in_ref),
                (gain_out_hbm, gain_out_ref),
            )
        )
    ]
    for copy in small:
        copy.start()
    weights = [
        pltpu.make_async_copy(src.at[0], dst, weight_sem.at[i])
        for i, (src, dst) in enumerate(
            ((w_gate_hbm, w_gate), (w_up_hbm, w_up), (w_down_hbm, w_down))
        )
    ]
    barrier = pltpu.get_barrier_semaphore()
    for step in range(1, experts):
        pl.semaphore_signal(
            barrier, inc=1, device_id={"ep": lax.rem(z + step, experts)}, device_id_type=MESH
        )
    for step in range(1, groups):
        pl.semaphore_signal(
            barrier, inc=1, device_id={"tp": lax.rem(q + step, groups)}, device_id_type=MESH
        )

    small[1].wait()
    small[2].wait()
    stage[...] = jnp.zeros_like(stage)
    stage[0:choose, :] = routes_ref[...].astype(jnp.float32)
    stage[choose : 2 * choose, :] = gates_ref[...]
    table[...] = jnp.transpose(stage[...])
    routes = table[:, 0:choose]
    lane = lax.broadcasted_iota(jnp.int32, (total, 128), 1).astype(jnp.float32)
    hit = ((routes[:, 0:1] == lane) | (routes[:, 1:2] == lane)).astype(jnp.float32)
    row_id = lax.broadcasted_iota(jnp.int32, (total, total), 0)
    col_id = lax.broadcasted_iota(jnp.int32, (total, total), 1)
    before = ((col_id < row_id) & (col_id // count == row_id // count)).astype(jnp.float32)
    earlier_ref[...] = jnp.dot(
        before.astype(jnp.bfloat16), hit.astype(jnp.bfloat16), preferred_element_type=jnp.float32
    )

    own = pl.ds(pl.multiple_of(q * count, count), count)
    own_routes = table[own, :]
    own_earlier = earlier_ref[own, :]
    own_lane = lax.broadcasted_iota(jnp.int32, (count, 128), 1).astype(jnp.float32)
    slots = lax.broadcasted_iota(jnp.int32, (count, experts * capacity), 1).astype(jnp.float32)
    select = jnp.zeros((count, experts * capacity), jnp.float32)
    for k in range(choose):
        expert = own_routes[:, k : k + 1]
        slot = jnp.sum(
            jnp.where(own_lane == expert, own_earlier, 0.0), axis=1, keepdims=True
        )
        select = jnp.where(slots == expert * capacity + slot, 1.0, select)

    small[0].wait()
    small[3].wait()
    values = tokens_ref[...].astype(jnp.float32)
    normed = (
        values
        * lax.rsqrt(jnp.mean(values * values, axis=-1, keepdims=True) + EPS)
        * gain_in_ref[...]
    ).astype(jnp.bfloat16)
    picked[...] = (
        lax.dot_general(
            select.astype(jnp.bfloat16),
            normed,
            (((0,), (0,)), ((), ())),
            preferred_element_type=jnp.float32,
        )
        .astype(jnp.bfloat16)
        .reshape(experts, capacity, width)
    )
    rows[z, q] = picked[z]

    pl.semaphore_wait(barrier, experts - 1 + groups - 1)

    sent = {}

    def remote(src, dst, send, recv, where):
        return pltpu.make_async_remote_copy(
            src_ref=src,
            dst_ref=dst,
            send_sem=send,
            recv_sem=recv,
            device_id=where,
            device_id_type=MESH,
        )

    def launch(make, *where):
        make(*where).start()
        sent[(make.__name__,) + where] = make

    def columns(h):
        return pl.ds(h * half_width, half_width)

    def lines(h):
        return pl.ds(h * half_rows, half_rows)

    def z_in(k, h, outward):
        there = peer[k]
        return remote(
            picked.at[there, :, columns(h)],
            rows.at[z if outward else there, q, :, columns(h)],
            d1_send.at[k, h],
            d1_recv.at[z if outward else there, h],
            {"ep": there},
        )

    def x_in(k, h):
        block = rows.at[peer[k], q, :, columns(h)]
        return remote(block, block, d2x_send.at[k, h], d2x_recv.at[k, h], {"tp": across})

    def pair_of(k, h):
        block = rows.at[peer[k], q, :, columns(h)]
        return remote(block, block, d2p_send.at[k, h], d2p_recv.at[k, h], {"tp": partner})

    def pair_across(k, h):
        block = rows.at[peer[k], across, :, columns(h)]
        return remote(block, block, d3_send.at[k, h], d3_recv.at[k, h], {"tp": partner})

    def spread(k, h):
        if k:
            z_in(k, h, False).wait_recv()
        launch(x_in, k, h)
        launch(pair_of, k, h)

    def relay(k, h):
        x_in(k, h).wait_recv()
        launch(pair_across, k, h)

    def pair_back(k, own_plane):
        there = plane if own_plane else 1 - plane
        return remote(
            part.at[k, there, 1 - core],
            pair_in.at[k, there],
            r1_send.at[k, own_plane],
            r1_recv.at[k, own_plane],
            {"tp": partner},
        )

    def x_back(k, h):
        return remote(
            cross_out.at[k, lines(h)],
            cross_in.at[k, lines(h)],
            r2_send.at[k, h],
            r2_recv.at[k, h],
            {"tp": across},
        )

    def z_back(k, h, outward):
        there = peer[k]
        where = z if outward else there
        return remote(
            home_out.at[k, lines(h)],
            home.at[where, lines(h)],
            r3_send.at[k, h],
            r3_recv.at[where, h],
            {"ep": there},
        )

    tile = 256
    tiles = hidden_width // tile

    def multiply(k, between):
        for h in range(2):
            pair_of(k, h).wait_recv()
            pair_across(k, h).wait_recv()
        x = rows[peer[k]].reshape(block_rows, width)
        for i in range(tiles):
            cols = pl.ds(i * tile, tile)
            gate = jnp.dot(x, w_gate[:, cols], preferred_element_type=jnp.float32)
            up = jnp.dot(x, w_up[:, cols], preferred_element_type=jnp.float32)
            hidden[:, cols] = (gate / (1.0 + jnp.exp(-gate)) * up).astype(jnp.bfloat16)
        for act in between:
            act()
        if k == 0:
            weights[2].wait()
        for own_plane in (0, 1):
            there = plane if own_plane else 1 - plane
            for c in range(2):
                cols = pl.ds(
                    pl.multiple_of((2 * there + c) * slice_width, slice_width), slice_width
                )
                product = jnp.dot(hidden[...], w_down[:, cols], preferred_element_type=jnp.float32)
                part[k, there, c] = product.astype(jnp.bfloat16)
            launch(pair_back, k, own_plane)

    def cross(k, h):
        other = 1 - plane
        if h == 0:
            pair_back(k, 0).wait_recv()
        cross_out[k, lines(h)] = (
            part[k, other, core, lines(h)].astype(jnp.float32)
            + pair_in[k, other, lines(h)].astype(jnp.float32)
        ).astype(jnp.bfloat16)
        launch(x_back, k, h)

    def give_back(k, h):
        if h == 0:
            pair_back(k, 1).wait_recv()
        x_back(k, h).wait_recv()
        result = (
            part[k, plane, core, lines(h)].astype(jnp.float32)
            + pair_in[k, plane, lines(h)].astype(jnp.float32)
            + cross_in[k, lines(h)].astype(jnp.float32)
        ).astype(jnp.bfloat16)
        if k == 0:
            home[z, lines(h)] = result
        else:
            home_out[k, lines(h)] = result
            launch(z_back, k, h, True)

    def join(k, h):
        z_back(k, h, False).wait_recv()

    def combine(k, first):
        if k:
            for h in range(2):
                join(k, h)
        e = peer[k]
        expert = e.astype(jnp.float32)
        mine = table[:, 0:choose] == expert
        lanes = lax.broadcasted_iota(jnp.int32, (total, 128), 1).astype(jnp.float32)
        slot = jnp.sum(jnp.where(lanes == expert, earlier_ref[...], 0.0), axis=1, keepdims=True)
        block = lax.broadcasted_iota(jnp.int32, (total, 1), 0) // count
        named = jnp.max(mine.astype(jnp.float32), axis=1, keepdims=True)
        target = jnp.where(
            named > 0.0, slot + (block * capacity).astype(jnp.float32), jnp.float32(-1.0)
        )
        weight = jnp.sum(jnp.where(mine, table[:, choose : 2 * choose], 0.0), axis=1, keepdims=True)
        place = lax.broadcasted_iota(jnp.int32, (total, block_rows), 1).astype(jnp.float32)
        pick = (place == target).astype(jnp.float32).astype(jnp.bfloat16)
        term = weight * jnp.dot(pick, home[e], preferred_element_type=jnp.float32)
        combined[...] = term if first else combined[...] + term

    def todo(act, *arguments, where=None):
        def run():
            if where is None:
                act(*arguments)
            else:
                pl.when(is_end if where == "end" else jnp.logical_not(is_end))(
                    lambda: act(*arguments)
                )

        return run

    def end(act, *arguments):
        return todo(act, *arguments, where="end")

    def middle(act, *arguments):
        return todo(act, *arguments, where="middle")

    def send(k):
        for h in range(2):
            launch(z_in, k, h, True)

    for h in range(2):
        spread(0, h)
    send(2)
    middle(send, 1)()
    middle(send, 3)()
    for copy in weights:
        copy.start()
    spread(1, 0)
    relay(0, 0)
    spread(1, 1)
    relay(0, 1)
    end(send, 1)()
    end(send, 3)()
    weights[0].wait()
    weights[1].wait()
    multiply(0, [todo(relay, 1, 0), end(spread, 2, 0)])
    middle(spread, 2, 0)()
    relay(1, 1)
    end(spread, 2, 1)()
    multiply(1, [middle(spread, 2, 1), end(relay, 2, 0)])
    middle(relay, 2, 0)()
    cross(1, 0)
    relay(2, 1)
    spread(3, 0)
    multiply(2, [todo(spread, 3, 1), todo(cross, 1, 1)])
    give_back(1, 0)
    cross(2, 0)
    cross(2, 1)
    relay(3, 0)
    relay(3, 1)
    multiply(3, [todo(give_back, 1, 1)])
    cross(3, 0)
    cross(3, 1)
    give_back(2, 0)
    cross(0, 0)
    cross(0, 1)
    give_back(2, 1)
    give_back(3, 0)
    give_back(3, 1)
    combine(2, True)
    combine(1, False)
    give_back(0, 0)
    give_back(0, 1)
    combine(0, False)
    combine(3, False)

    small[4].wait()
    value = combined[...]
    ones = jnp.ones((8, slice_width), jnp.float32)
    squares[q] = lax.dot_general(
        ones,
        value * value,
        (((1,), (1,)), ((), ())),
        preferred_element_type=jnp.float32,
        precision=lax.Precision.HIGHEST,
    )

    def share(step):
        return remote(
            squares.at[q],
            squares.at[q],
            sq_send.at[step],
            sq_recv.at[step],
            {"tp": lax.rem(q + step, groups)},
        )

    for step in range(1, groups):
        launch(share, step)
    for step in range(1, groups):
        share(step).wait_recv()
    summed = squares[0]
    for i in range(1, groups):
        summed = summed + squares[i]
    scale = lax.rsqrt(summed / width + EPS)
    column = jnp.transpose(scale)[:, 0:1]
    out_ref[...] = (combined[...] * column * gain_out_ref[...]).astype(jnp.bfloat16)
    for key, make in sent.items():
        make(*key[1:]).wait_send()


def fused(tokens, gain_in, routes, gates, w_gate, w_up, w_down, gain_out, capacity):
    experts = lax.axis_size("ep")
    groups = lax.axis_size("tp")
    count, width = tokens.shape
    total = routes.shape[0]
    hidden_width = w_gate.shape[2]
    slice_width = width // groups
    block_rows = groups * capacity
    bf16, f32 = jnp.bfloat16, jnp.float32
    vmem = pl.BlockSpec(memory_space=pltpu.VMEM)
    hbm = pl.BlockSpec(memory_space=pl.ANY)
    dma = pltpu.SemaphoreType.DMA
    return pl.pallas_call(
        functools.partial(fused_kernel, experts, groups, capacity),
        out_shape=jax.ShapeDtypeStruct((total, slice_width), bf16),
        in_specs=[hbm] * 8,
        out_specs=vmem,
        scratch_shapes=[
            pltpu.VMEM(tokens.shape, bf16),
            pltpu.VMEM((1, width), f32),
            pltpu.VMEM((routes.shape[1], total), jnp.int32),
            pltpu.VMEM((routes.shape[1], total), f32),
            pltpu.VMEM((1, slice_width), f32),
            pltpu.VMEM((8, total), f32),
            pltpu.VMEM((total, 8), f32),
            pltpu.VMEM((width, hidden_width), bf16),
            pltpu.VMEM((width, hidden_width), bf16),
            pltpu.VMEM((hidden_width, width), bf16),
            pltpu.VMEM((total, 128), f32),
            pltpu.VMEM((experts, capacity, width), bf16),
            pltpu.VMEM((experts, groups, capacity, width), bf16),
            pltpu.VMEM((block_rows, hidden_width), bf16),
            pltpu.VMEM((experts, groups // 2, 2, block_rows, slice_width), bf16),
            pltpu.VMEM((experts, groups // 2, block_rows, slice_width), bf16),
            pltpu.VMEM((experts, block_rows, slice_width), bf16),
            pltpu.VMEM((experts, block_rows, slice_width), bf16),
            pltpu.VMEM((experts, block_rows, slice_width), bf16),
            pltpu.VMEM((experts, block_rows, slice_width), bf16),
            pltpu.VMEM((total, slice_width), f32),
            pltpu.VMEM((groups, 8, total), f32),
            dma((3,)),
            dma((5,)),
        ]
        + [dma((experts, 2)) for _ in range(14)]
        + [dma((groups,)) for _ in range(2)],
        compiler_params=pltpu.CompilerParams(
            collective_id=0, has_side_effects=True, vmem_limit_bytes=60 * 1024 * 1024
        ),
    )(tokens, gain_in[None], routes.T, gates.T, w_gate, w_up, w_down, gain_out[None])


def local(tokens, gain_in, routes, gates, w_gate, w_up, w_down, gain_out):
    count, width = tokens.shape
    choose = routes.shape[1]
    experts = lax.axis_size("ep")
    groups = lax.axis_size("tp")
    capacity = (3 * count * choose + 2 * experts - 1) // (2 * experts)
    hidden_width = w_gate.shape[2]
    if experts == 4 and groups == 4 and choose == 2 and capacity % 16 == 0 and hidden_width % 256 == 0:
        return fused(
            tokens, gain_in, routes, gates, w_gate, w_up, w_down, gain_out, capacity
        )
    values = tokens.astype(jnp.float32)
    normed = (
        values * lax.rsqrt(jnp.mean(values * values, axis=-1, keepdims=True) + EPS) * gain_in
    ).astype(jnp.bfloat16)
    positions = slot_table(routes.reshape(groups, count, choose), experts, capacity)
    own = lax.dynamic_index_in_dim(positions, lax.axis_index("tp"), 0, keepdims=False)
    slots = jnp.arange(experts * capacity, dtype=jnp.int32)
    select = jnp.sum((own[None, :, :] == slots[:, None, None]).astype(jnp.bfloat16), axis=2)
    outgoing = jnp.dot(select, normed, preferred_element_type=jnp.float32).astype(jnp.bfloat16)
    outgoing = outgoing.reshape(experts, capacity, width)
    arrived = lax.all_to_all(outgoing, "ep", split_axis=0, concat_axis=0, tiled=True)
    piece = lax.all_gather(arrived[:, None], "tp", axis=1, tiled=True)
    flat = piece.reshape(-1, width)
    gate = jnp.dot(flat, w_gate[0], preferred_element_type=jnp.float32)
    up = jnp.dot(flat, w_up[0], preferred_element_type=jnp.float32)
    hidden = (jax.nn.silu(gate) * up).astype(jnp.bfloat16)
    hidden = hidden.reshape(piece.shape[:-1] + (hidden_width,))
    partial_value = jnp.dot(
        hidden.reshape(-1, hidden_width), w_down[0], preferred_element_type=jnp.float32
    )
    summed = lax.psum_scatter(
        partial_value.astype(jnp.bfloat16), "tp", scatter_dimension=1, tiled=True
    )
    slice_width = width // groups
    expert_out = summed.reshape(experts, groups * capacity, slice_width)
    returned = lax.all_to_all(expert_out, "ep", split_axis=0, concat_axis=0, tiled=True)
    returned = returned.reshape(experts, groups, capacity, slice_width).transpose(1, 0, 2, 3)
    returned = returned.reshape(groups, experts * capacity, slice_width).astype(jnp.float32)
    weights = gates.reshape(groups, count, choose)
    combine = jnp.sum(
        jnp.where(
            positions[..., None] == slots[None, None, None, :], weights[..., None], jnp.float32(0.0)
        ),
        axis=2,
    )
    combined = jnp.einsum("gtp,gpd->gtd", combine, returned, precision=lax.Precision.HIGHEST)
    combined = combined.reshape(groups * count, slice_width)
    squares = lax.psum(jnp.sum(combined * combined, axis=1), "tp")
    scale = lax.rsqrt(squares / width + EPS)
    return (combined * scale[:, None] * gain_out).astype(jnp.bfloat16)


def solution(mesh):
    in_specs = (
        P(("grp", "ep", "tp"), None),
        P(),
        P(("grp", "ep"), None),
        P(("grp", "ep"), None),
        P("ep", None, "tp"),
        P("ep", None, "tp"),
        P("ep", "tp", None),
        P("tp"),
    )
    out_specs = P(("grp", "ep"), "tp")
    return jax.shard_map(local, mesh=mesh, in_specs=in_specs, out_specs=out_specs, check_vma=False)
```

profile of v0, /device:TPU:0, one launch (start us, length us, event | category | flops | bytes accessed | tf_op | source)
XLA Modules:
  0.0 55.1 jit_solution(248206907082823788)
XLA Ops:
  0.0 53.4 %shard_map.82 = bf16[256,512]{1,0:T(8,128)(2,1)} custom-call(bf16[64,2048]{1,0:T(8,128)(2,1)} %tokens_hbm.1, f32[1,2048]{1,0:T(1,128)} %bitcast.4, s32[2,256]{1,0:T(2,128)} %bitcast.5, f32[2,256]{1,0:T(2,128)} %bitcast.6, bf16[1,2048,768]{2,1,0:T(8,128)(2,1)} %w_gate_hbm.1, bf16[1,2048,768]{2,1,0:T(8,128)(2,1)} %w_up_hbm.1, ...), custom_call_target="tpu_custom_call" | custom-call | tf_op jit(solution)/shard_map/pallas_call | solution.py:456
  53.4 1.7 %copy.10 = bf16[256,512]{1,0:T(8,128)(2,1)} copy(bf16[256,512]{1,0:T(8,128)(2,1)} %shard_map.82) | data formatting | bytes 524288
where the time goes:
time: 55.8 us; the launch traced here: 55.1 us
  Pallas kernels  53.4 us (96%)
  local copies, waits for them, and re-layouts  1.67 us (3%)
    pallas_call x1, Pallas kernels, fused(): pl.pallas_call(functools.partial(fused_kernel, experts, groups, capacity)...  53.4 us
    unnamed x1, local copies, waits for them, and re-layouts  1.67 us

commit v1 on v0

--- a/solution.py
+++ b/solution.py
@@ -90,13 +90,15 @@
     hidden_width = w_gate.shape[1]
     slice_width = out_ref.shape[1]
     block_rows = groups * capacity
-    half_width = width // 2
-    half_rows = block_rows // 2
+    pieces = d1_recv.shape[1]
+    per_half = pieces // 2
+    piece_width = width // pieces
+    piece_rows = block_rows // pieces
 
     last = experts - 1
     side = z // 2
     inward = z + side * (last - 2 * z)
-    near = [inward, 2 - 2 * inward, 1 + 2 * inward, last - inward]
+    near = [inward, 2 - 2 * inward, 1 + inward, last + 0 * inward]
     peer = [p + side * (last - 2 * p) for p in near]
     is_end = inward == 0
 
@@ -136,20 +138,17 @@
     stage[0:choose, :] = routes_ref[...].astype(jnp.float32)
     stage[choose : 2 * choose, :] = gates_ref[...]
     table[...] = jnp.transpose(stage[...])
-    routes = table[:, 0:choose]
-    lane = lax.broadcasted_iota(jnp.int32, (total, 128), 1).astype(jnp.float32)
-    hit = ((routes[:, 0:1] == lane) | (routes[:, 1:2] == lane)).astype(jnp.float32)
-    row_id = lax.broadcasted_iota(jnp.int32, (total, total), 0)
-    col_id = lax.broadcasted_iota(jnp.int32, (total, total), 1)
-    before = ((col_id < row_id) & (col_id // count == row_id // count)).astype(jnp.float32)
-    earlier_ref[...] = jnp.dot(
-        before.astype(jnp.bfloat16), hit.astype(jnp.bfloat16), preferred_element_type=jnp.float32
-    )
-
     own = pl.ds(pl.multiple_of(q * count, count), count)
     own_routes = table[own, :]
-    own_earlier = earlier_ref[own, :]
     own_lane = lax.broadcasted_iota(jnp.int32, (count, 128), 1).astype(jnp.float32)
+    own_hit = (own_routes[:, 0:1] == own_lane) | (own_routes[:, 1:2] == own_lane)
+    own_row = lax.broadcasted_iota(jnp.int32, (count, count), 0)
+    own_col = lax.broadcasted_iota(jnp.int32, (count, count), 1)
+    own_earlier = jnp.dot(
+        (own_col < own_row).astype(jnp.float32).astype(jnp.bfloat16),
+        own_hit.astype(jnp.float32).astype(jnp.bfloat16),
+        preferred_element_type=jnp.float32,
+    )
     slots = lax.broadcasted_iota(jnp.int32, (count, experts * capacity), 1).astype(jnp.float32)
     select = jnp.zeros((count, experts * capacity), jnp.float32)
     for k in range(choose):
@@ -181,8 +180,6 @@
 
     pl.semaphore_wait(barrier, experts - 1 + groups - 1)
 
-    sent = {}
-
     def remote(src, dst, send, recv, where):
         return pltpu.make_async_remote_copy(
             src_ref=src,
@@ -193,54 +190,56 @@
             device_id_type=MESH,
         )
 
-    def launch(make, *where):
-        make(*where).start()
-        sent[(make.__name__,) + where] = make
-
     def columns(h):
-        return pl.ds(h * half_width, half_width)
+        return pl.ds(h * piece_width, piece_width)
 
     def lines(h):
-        return pl.ds(h * half_rows, half_rows)
+        return pl.ds(h * piece_rows, piece_rows)
+
+    def in_half(half):
+        return range(half * per_half, (half + 1) * per_half)
 
     def z_in(k, h, outward):
         there = peer[k]
+        where = z if outward else there
         return remote(
             picked.at[there, :, columns(h)],
-            rows.at[z if outward else there, q, :, columns(h)],
-            d1_send.at[k, h],
-            d1_recv.at[z if outward else there, h],
+            rows.at[where, q, :, columns(h)],
+            d1_send.at[0],
+            d1_recv.at[where, h],
             {"ep": there},
         )
 
     def x_in(k, h):
         block = rows.at[peer[k], q, :, columns(h)]
-        return remote(block, block, d2x_send.at[k, h], d2x_recv.at[k, h], {"tp": across})
-
-    def pair_of(k, h):
-        block = rows.at[peer[k], q, :, columns(h)]
-        return remote(block, block, d2p_send.at[k, h], d2p_recv.at[k, h], {"tp": partner})
-
-    def pair_across(k, h):
-        block = rows.at[peer[k], across, :, columns(h)]
-        return remote(block, block, d3_send.at[k, h], d3_recv.at[k, h], {"tp": partner})
-
-    def spread(k, h):
-        if k:
-            z_in(k, h, False).wait_recv()
-        launch(x_in, k, h)
-        launch(pair_of, k, h)
-
-    def relay(k, h):
-        x_in(k, h).wait_recv()
-        launch(pair_across, k, h)
+        return remote(block, block, d2x_send.at[0], d2x_recv.at[k, h], {"tp": across})
+
+    def pair_of(k, cols):
+        block = rows.at[peer[k], q, :, cols]
+        return remote(block, block, d2p_send.at[0], d2p_recv.at[k], {"tp": partner})
+
+    def pair_across(k, cols):
+        block = rows.at[peer[k], across, :, cols]
+        return remote(block, block, d3_send.at[0], d3_recv.at[k], {"tp": partner})
+
+    def spread(k, half):
+        for h in in_half(half):
+            if k:
+                z_in(k, h, False).wait_recv()
+            x_in(k, h).start()
+            pair_of(k, columns(h)).start()
+
+    def relay(k, half):
+        for h in in_half(half):
+            x_in(k, h).wait_recv()
+            pair_across(k, columns(h)).start()
 
     def pair_back(k, own_plane):
         there = plane if own_plane else 1 - plane
         return remote(
             part.at[k, there, 1 - core],
             pair_in.at[k, there],
-            r1_send.at[k, own_plane],
+            r1_send.at[0],
             r1_recv.at[k, own_plane],
             {"tp": partner},
         )
@@ -249,19 +248,19 @@
         return remote(
             cross_out.at[k, lines(h)],
             cross_in.at[k, lines(h)],
-            r2_send.at[k, h],
+            r2_send.at[0],
             r2_recv.at[k, h],
             {"tp": across},
         )
 
-    def z_back(k, h, outward):
+    def z_back(k, rows_of, outward):
         there = peer[k]
         where = z if outward else there
         return remote(
-            home_out.at[k, lines(h)],
-            home.at[where, lines(h)],
-            r3_send.at[k, h],
-            r3_recv.at[where, h],
+            home_out.at[k, rows_of],
+            home.at[where, rows_of],
+            r3_send.at[0],
+            r3_recv.at[where],
             {"ep": there},
         )
 
@@ -269,9 +268,9 @@
     tiles = hidden_width // tile
 
     def multiply(k, between):
-        for h in range(2):
-            pair_of(k, h).wait_recv()
-            pair_across(k, h).wait_recv()
+        every = pl.ds(0, width)
+        pair_of(k, every).wait_recv()
+        pair_across(k, every).wait_recv()
         x = rows[peer[k]].reshape(block_rows, width)
         for i in range(tiles):
             cols = pl.ds(i * tile, tile)
@@ -290,40 +289,54 @@
                 )
                 product = jnp.dot(hidden[...], w_down[:, cols], preferred_element_type=jnp.float32)
                 part[k, there, c] = product.astype(jnp.bfloat16)
-            launch(pair_back, k, own_plane)
-
-    def cross(k, h):
+            pair_back(k, own_plane).start()
+
+    def cross(k, half):
         other = 1 - plane
-        if h == 0:
+        if half == 0:
             pair_back(k, 0).wait_recv()
-        cross_out[k, lines(h)] = (
-            part[k, other, core, lines(h)].astype(jnp.float32)
-            + pair_in[k, other, lines(h)].astype(jnp.float32)
-        ).astype(jnp.bfloat16)
-        launch(x_back, k, h)
-
-    def give_back(k, h):
-        if h == 0:
+        for h in in_half(half):
+            cross_out[k, lines(h)] = (
+                part[k, other, core, lines(h)].astype(jnp.float32)
+                + pair_in[k, other, lines(h)].astype(jnp.float32)
+            ).astype(jnp.bfloat16)
+            x_back(k, h).start()
+
+    def give_back(k, half):
+        if half == 0:
             pair_back(k, 1).wait_recv()
-        x_back(k, h).wait_recv()
-        result = (
-            part[k, plane, core, lines(h)].astype(jnp.float32)
-            + pair_in[k, plane, lines(h)].astype(jnp.float32)
-            + cross_in[k, lines(h)].astype(jnp.float32)
-        ).astype(jnp.bfloat16)
-        if k == 0:
-            home[z, lines(h)] = result
-        else:
-            home_out[k, lines(h)] = result
-            launch(z_back, k, h, True)
-
-    def join(k, h):
-        z_back(k, h, False).wait_recv()
+        for h in in_half(half):
+            x_back(k, h).wait_recv()
+            result = (
+                part[k, plane, core, lines(h)].astype(jnp.float32)
+                + pair_in[k, plane, lines(h)].astype(jnp.float32)
+                + cross_in[k, lines(h)].astype(jnp.float32)
+            ).astype(jnp.bfloat16)
+            if k == 0:
+                home[z, lines(h)] = result
+            else:
+                home_out[k, lines(h)] = result
+                z_back(k, lines(h), True).start()
+
+    def count_earlier():
+        routes = table[:, 0:choose]
+        lane = lax.broadcasted_iota(jnp.int32, (total, 128), 1).astype(jnp.float32)
+        hit = ((routes[:, 0:1] == lane) | (routes[:, 1:2] == lane)).astype(jnp.float32)
+        row_id = lax.broadcasted_iota(jnp.int32, (total, total), 0)
+        col_id = lax.broadcasted_iota(jnp.int32, (total, total), 1)
+        before = ((col_id < row_id) & (col_id // count == row_id // count)).astype(jnp.float32)
+        earlier_ref[...] = jnp.dot(
+            before.astype(jnp.bfloat16),
+            hit.astype(jnp.bfloat16),
+            preferred_element_type=jnp.float32,
+        )
+
+    def join(k):
+        z_back(k, pl.ds(0, block_rows), False).wait_recv()
 
     def combine(k, first):
         if k:
-            for h in range(2):
-                join(k, h)
+            join(k)
         e = peer[k]
         expert = e.astype(jnp.float32)
         mine = table[:, 0:choose] == expert
@@ -358,87 +371,105 @@
         return todo(act, *arguments, where="middle")
 
     def send(k):
-        for h in range(2):
-            launch(z_in, k, h, True)
+        for h in range(pieces):
+            z_in(k, h, True).start()
 
     for h in range(2):
         spread(0, h)
-    send(2)
+    end(send, 2)()
+    middle(send, 3)()
     middle(send, 1)()
-    middle(send, 3)()
+    middle(send, 2)()
     for copy in weights:
         copy.start()
+    count_earlier()
     spread(1, 0)
     relay(0, 0)
     spread(1, 1)
     relay(0, 1)
-    end(send, 1)()
-    end(send, 3)()
     weights[0].wait()
     weights[1].wait()
-    multiply(0, [todo(relay, 1, 0), end(spread, 2, 0)])
-    middle(spread, 2, 0)()
+    multiply(0, [end(send, 1), end(send, 3), todo(spread, 2, 0)])
+    relay(1, 0)
     relay(1, 1)
-    end(spread, 2, 1)()
-    multiply(1, [middle(spread, 2, 1), end(relay, 2, 0)])
-    middle(relay, 2, 0)()
+    spread(2, 1)
+    cross(0, 0)
+    multiply(1, [todo(relay, 2, 0)])
+    relay(2, 1)
     cross(1, 0)
-    relay(2, 1)
-    spread(3, 0)
-    multiply(2, [todo(spread, 3, 1), todo(cross, 1, 1)])
-    give_back(1, 0)
+    end(cross, 1, 1)()
+    middle(spread, 3, 0)()
+    multiply(2, [middle(spread, 3, 1)])
+    end(spread, 3, 0)()
+    end(give_back, 1, 0)()
+    end(spread, 3, 1)()
+    end(give_back, 1, 1)()
+    middle(cross, 1, 1)()
     cross(2, 0)
     cross(2, 1)
+    middle(give_back, 1, 0)()
     relay(3, 0)
     relay(3, 1)
-    multiply(3, [todo(give_back, 1, 1)])
+    multiply(3, [end(give_back, 2, 0), middle(give_back, 1, 1)])
     cross(3, 0)
     cross(3, 1)
-    give_back(2, 0)
-    cross(0, 0)
+    middle(give_back, 2, 0)()
+    give_back(2, 1)
     cross(0, 1)
-    give_back(2, 1)
     give_back(3, 0)
     give_back(3, 1)
     combine(2, True)
-    combine(1, False)
     give_back(0, 0)
     give_back(0, 1)
     combine(0, False)
+    combine(1, False)
     combine(3, False)
 
     small[4].wait()
     value = combined[...]
-    ones = jnp.ones((8, slice_width), jnp.float32)
+    folded = sum(
+        value[:, i : i + 128] * value[:, i : i + 128] for i in range(0, slice_width, 128)
+    )
+    ones = jnp.ones((8, 128), jnp.float32)
     squares[q] = lax.dot_general(
         ones,
-        value * value,
+        folded,
         (((1,), (1,)), ((), ())),
         preferred_element_type=jnp.float32,
         precision=lax.Precision.HIGHEST,
     )
 
-    def share(step):
+    def share(step, rows_of):
         return remote(
-            squares.at[q],
-            squares.at[q],
-            sq_send.at[step],
+            squares.at[rows_of],
+            squares.at[rows_of],
+            sq_send.at[0],
             sq_recv.at[step],
             {"tp": lax.rem(q + step, groups)},
         )
 
     for step in range(1, groups):
-        launch(share, step)
+        share(step, pl.ds(q, 1)).start()
     for step in range(1, groups):
-        share(step).wait_recv()
+        share(step, pl.ds(q, 1)).wait_recv()
     summed = squares[0]
     for i in range(1, groups):
         summed = summed + squares[i]
     scale = lax.rsqrt(summed / width + EPS)
     column = jnp.transpose(scale)[:, 0:1]
     out_ref[...] = (combined[...] * column * gain_out_ref[...]).astype(jnp.bfloat16)
-    for key, make in sent.items():
-        make(*key[1:]).wait_send()
+
+    def drain(block, semaphore):
+        remote(block, block, semaphore.at[0], semaphore.at[0], {"tp": across}).wait_send()
+
+    drain(picked.at[0 : experts - 1], d1_send)
+    drain(rows.at[0], d2x_send)
+    drain(rows.at[0], d2p_send)
+    drain(rows.at[0], d3_send)
+    drain(pair_in, r1_send)
+    drain(cross_out, r2_send)
+    drain(home_out.at[1:experts], r3_send)
+    drain(squares.at[1:groups], sq_send)
 
 
 def fused(tokens, gain_in, routes, gates, w_gate, w_up, w_down, gain_out, capacity):
@@ -483,13 +514,41 @@
             pltpu.VMEM((groups, 8, total), f32),
             dma((3,)),
             dma((5,)),
-        ]
-        + [dma((experts, 2)) for _ in range(14)]
-        + [dma((groups,)) for _ in range(2)],
+            dma((1,)),
+            dma((experts, 4)),
+            dma((1,)),
+            dma((experts,)),
+            dma((1,)),
+            dma((experts, 4)),
+            dma((1,)),
+            dma((experts,)),
+            dma((1,)),
+            dma((experts, 2)),
+            dma((1,)),
+            dma((experts, 4)),
+            dma((1,)),
+            dma((experts,)),
+            dma((1,)),
+            dma((groups,)),
+        ],
         compiler_params=pltpu.CompilerParams(
-            collective_id=0, has_side_effects=True, vmem_limit_bytes=60 * 1024 * 1024
+            collective_id=0, has_side_effects=True, vmem_limit_bytes=48000 * 1024
         ),
-    )(tokens, gain_in[None], routes.T, gates.T, w_gate, w_up, w_down, gain_out[None])
+    )(
+        *(
+            pltpu.with_memory_space_constraint(array, pltpu.HBM)
+            for array in (
+                tokens,
+                gain_in[None],
+                routes.T,
+                gates.T,
+                w_gate,
+                w_up,
+                w_down,
+                gain_out[None],
+            )
+        )
+    )
 
 
 def local(tokens, gain_in, routes, gates, w_gate, w_up, w_down, gain_out):

time: 55.8 us -> 53.1 us (0.952); the launches traced: 55.1 us -> 53 us
  Pallas kernels: 53.4 us -> 52.3 us
  local copies, waits for them, and re-layouts: 1.67 us -> 0.71 us
    pallas_call x1, Pallas kernels: 53.4 us -> 52.3 us  [fused(): pl.pallas_call(functools.partial(fused_kernel, experts, groups, capacity)...]
    unnamed x1, local copies, waits for them, and re-layouts: 1.67 us -> 0.71 us
where the time goes in v1:
time: 53.1 us; the launch traced here: 53 us
  Pallas kernels  52.3 us (98%)
  local copies, waits for them, and re-layouts  0.71 us (1%)
    pallas_call x1, Pallas kernels, fused(): pl.pallas_call(functools.partial(fused_kernel, experts, groups, capacity)...  52.3 us

profile of v1, /device:TPU:0, one launch (start us, length us, event | category | flops | bytes accessed | tf_op | source)
XLA Modules:
  0.0 53.0 jit_solution(6862528187603300304)
XLA Ops:
  0.0 52.3 %shard_map.82 = bf16[256,512]{1,0:T(8,128)(2,1)S(1)} custom-call(bf16[64,2048]{1,0:T(8,128)(2,1)} %tokens_hbm.1, f32[1,2048]{1,0:T(1,128)} %bitcast.4, s32[2,256]{1,0:T(2,128)} %bitcast.5, f32[2,256]{1,0:T(2,128)} %bitcast.6, bf16[1,2048,768]{2,1,0:T(8,128)(2,1)} %w_gate_hbm.1, bf16[1,2048,768]{2,1,0:T(8,128)(2,1)} %w_up_hbm.1, ...), custom_call_target="tpu_custom_call" | custom-call | tf_op jit(solution)/shard_map/pallas_call | solution.py:487
  52.3 0.7 %copy.10 = bf16[256,512]{1,0:T(8,128)(2,1)} copy(bf16[256,512]{1,0:T(8,128)(2,1)S(1)} %shard_map.82) | data formatting | bytes 524288

commit v2 on v1

--- a/solution.py
+++ b/solution.py
@@ -58,6 +58,8 @@
     home_out,
     home,
     combined,
+    gate_sum,
+    up_sum,
     squares,
     weight_sem,
     small_sem,
@@ -132,8 +134,8 @@
             barrier, inc=1, device_id={"tp": lax.rem(q + step, groups)}, device_id_type=MESH
         )
 
-    small[1].wait()
-    small[2].wait()
+    for i in (1, 2, 0, 3):
+        small[i].wait()
     stage[...] = jnp.zeros_like(stage)
     stage[0:choose, :] = routes_ref[...].astype(jnp.float32)
     stage[choose : 2 * choose, :] = gates_ref[...]
@@ -158,8 +160,6 @@
         )
         select = jnp.where(slots == expert * capacity + slot, 1.0, select)
 
-    small[0].wait()
-    small[3].wait()
     values = tokens_ref[...].astype(jnp.float32)
     normed = (
         values
@@ -214,25 +214,25 @@
         block = rows.at[peer[k], q, :, columns(h)]
         return remote(block, block, d2x_send.at[0], d2x_recv.at[k, h], {"tp": across})
 
-    def pair_of(k, cols):
+    def pair_of(k, cols, h):
         block = rows.at[peer[k], q, :, cols]
-        return remote(block, block, d2p_send.at[0], d2p_recv.at[k], {"tp": partner})
-
-    def pair_across(k, cols):
+        return remote(block, block, d2p_send.at[0], d2p_recv.at[k, h // per_half], {"tp": partner})
+
+    def pair_across(k, cols, h):
         block = rows.at[peer[k], across, :, cols]
-        return remote(block, block, d3_send.at[0], d3_recv.at[k], {"tp": partner})
+        return remote(block, block, d3_send.at[0], d3_recv.at[k, h // per_half], {"tp": partner})
 
     def spread(k, half):
         for h in in_half(half):
             if k:
                 z_in(k, h, False).wait_recv()
             x_in(k, h).start()
-            pair_of(k, columns(h)).start()
+            pair_of(k, columns(h), h).start()
 
     def relay(k, half):
         for h in in_half(half):
             x_in(k, h).wait_recv()
-            pair_across(k, columns(h)).start()
+            pair_across(k, columns(h), h).start()
 
     def pair_back(k, own_plane):
         there = plane if own_plane else 1 - plane
@@ -267,15 +267,38 @@
     tile = 256
     tiles = hidden_width // tile
 
-    def multiply(k, between):
-        every = pl.ds(0, width)
-        pair_of(k, every).wait_recv()
-        pair_across(k, every).wait_recv()
-        x = rows[peer[k]].reshape(block_rows, width)
+    half_width = width // 2
+
+    def landed(k, half):
+        cols = pl.ds(half * half_width, half_width)
+        pair_of(k, cols, half * per_half).wait_recv()
+        pair_across(k, cols, half * per_half).wait_recv()
+
+    def begin(k):
+        landed(k, 0)
+        x = rows[peer[k], :, :, 0:half_width].reshape(block_rows, half_width)
         for i in range(tiles):
             cols = pl.ds(i * tile, tile)
-            gate = jnp.dot(x, w_gate[:, cols], preferred_element_type=jnp.float32)
-            up = jnp.dot(x, w_up[:, cols], preferred_element_type=jnp.float32)
+            gate_sum[:, cols] = jnp.dot(
+                x, w_gate[0:half_width, cols], preferred_element_type=jnp.float32
+            )
+            up_sum[:, cols] = jnp.dot(
+                x, w_up[0:half_width, cols], preferred_element_type=jnp.float32
+            )
+
+    def multiply(k, between, begun=False):
+        if not begun:
+            landed(k, 0)
+        landed(k, 1)
+        start = half_width if begun else 0
+        x = rows[peer[k], :, :, start:width].reshape(block_rows, width - start)
+        for i in range(tiles):
+            cols = pl.ds(i * tile, tile)
+            gate = jnp.dot(x, w_gate[start:width, cols], preferred_element_type=jnp.float32)
+            up = jnp.dot(x, w_up[start:width, cols], preferred_element_type=jnp.float32)
+            if begun:
+                gate = gate + gate_sum[:, cols]
+                up = up + up_sum[:, cols]
             hidden[:, cols] = (gate / (1.0 + jnp.exp(-gate)) * up).astype(jnp.bfloat16)
         for act in between:
             act()
@@ -393,28 +416,29 @@
     relay(1, 0)
     relay(1, 1)
     spread(2, 1)
-    cross(0, 0)
-    multiply(1, [todo(relay, 2, 0)])
+    end(cross, 0, 0)()
+    multiply(1, [todo(relay, 2, 0), middle(spread, 3, 0)])
     relay(2, 1)
+    middle(spread, 3, 1)()
     cross(1, 0)
-    end(cross, 1, 1)()
-    middle(spread, 3, 0)()
-    multiply(2, [middle(spread, 3, 1)])
-    end(spread, 3, 0)()
+    cross(1, 1)
+    multiply(2, [middle(relay, 3, 0), end(spread, 3, 0)])
+    end(spread, 3, 1)()
     end(give_back, 1, 0)()
-    end(spread, 3, 1)()
     end(give_back, 1, 1)()
-    middle(cross, 1, 1)()
+    middle(relay, 3, 1)()
     cross(2, 0)
     cross(2, 1)
     middle(give_back, 1, 0)()
-    relay(3, 0)
-    relay(3, 1)
-    multiply(3, [end(give_back, 2, 0), middle(give_back, 1, 1)])
+    end(relay, 3, 0)()
+    begin(3)
+    end(relay, 3, 1)()
+    multiply(3, [middle(give_back, 1, 1)], True)
     cross(3, 0)
     cross(3, 1)
-    middle(give_back, 2, 0)()
+    give_back(2, 0)
     give_back(2, 1)
+    middle(cross, 0, 0)()
     cross(0, 1)
     give_back(3, 0)
     give_back(3, 1)
@@ -511,17 +535,19 @@
             pltpu.VMEM((experts, block_rows, slice_width), bf16),
             pltpu.VMEM((experts, block_rows, slice_width), bf16),
             pltpu.VMEM((total, slice_width), f32),
+            pltpu.VMEM((block_rows, hidden_width), f32),
+            pltpu.VMEM((block_rows, hidden_width), f32),
             pltpu.VMEM((groups, 8, total), f32),
             dma((3,)),
             dma((5,)),
             dma((1,)),
             dma((experts, 4)),
             dma((1,)),
-            dma((experts,)),
+            dma((experts, 2)),
             dma((1,)),
             dma((experts, 4)),
             dma((1,)),
-            dma((experts,)),
+            dma((experts, 2)),
             dma((1,)),
             dma((experts, 2)),
             dma((1,)),

time: 53.1 us -> 51.8 us (0.976)
  Pallas kernels: 52.3 us -> 50.9 us
    pallas_call x1, Pallas kernels: 52.3 us -> 50.9 us  [fused(): pl.pallas_call(functools.partial(fused_kernel, experts, groups, capacity)...]
where the time goes in v2:
time: 51.8 us; the launch traced here: 51.6 us
  Pallas kernels  50.9 us (98%)
  local copies, waits for them, and re-layouts  0.71 us (1%)
    pallas_call x1, Pallas kernels, fused(): pl.pallas_call(functools.partial(fused_kernel, experts, groups, capacity)...  50.9 us

profile of v2, /device:TPU:0, one launch (start us, length us, event | category | flops | bytes accessed | tf_op | source)
XLA Modules:
  0.0 51.6 jit_solution(10836857769320813452)
XLA Ops:
  0.0 50.9 %shard_map.82 = bf16[256,512]{1,0:T(8,128)(2,1)S(1)} custom-call(bf16[64,2048]{1,0:T(8,128)(2,1)} %tokens_hbm.1, f32[1,2048]{1,0:T(1,128)} %bitcast.4, s32[2,256]{1,0:T(2,128)} %bitcast.5, f32[2,256]{1,0:T(2,128)} %bitcast.6, bf16[1,2048,768]{2,1,0:T(8,128)(2,1)} %w_gate_hbm.1, bf16[1,2048,768]{2,1,0:T(8,128)(2,1)} %w_up_hbm.1, ...), custom_call_target="tpu_custom_call" | custom-call | tf_op jit(solution)/shard_map/pallas_call | solution.py:511
  50.9 0.7 %copy.10 = bf16[256,512]{1,0:T(8,128)(2,1)} copy(bf16[256,512]{1,0:T(8,128)(2,1)S(1)} %shard_map.82) | data formatting | bytes 524288

commit v3 on v2

--- a/solution.py
+++ b/solution.py
@@ -358,8 +358,6 @@
         z_back(k, pl.ds(0, block_rows), False).wait_recv()
 
     def combine(k, first):
-        if k:
-            join(k)
         e = peer[k]
         expert = e.astype(jnp.float32)
         mine = table[:, 0:choose] == expert
@@ -373,6 +371,8 @@
         weight = jnp.sum(jnp.where(mine, table[:, choose : 2 * choose], 0.0), axis=1, keepdims=True)
         place = lax.broadcasted_iota(jnp.int32, (total, block_rows), 1).astype(jnp.float32)
         pick = (place == target).astype(jnp.float32).astype(jnp.bfloat16)
+        if k:
+            join(k)
         term = weight * jnp.dot(pick, home[e], preferred_element_type=jnp.float32)
         combined[...] = term if first else combined[...] + term
 
@@ -422,9 +422,10 @@
     middle(spread, 3, 1)()
     cross(1, 0)
     cross(1, 1)
-    multiply(2, [middle(relay, 3, 0), end(spread, 3, 0)])
+    multiply(2, [middle(relay, 3, 0)])
+    end(spread, 3, 0)()
+    end(give_back, 1, 0)()
     end(spread, 3, 1)()
-    end(give_back, 1, 0)()
     end(give_back, 1, 1)()
     middle(relay, 3, 1)()
     cross(2, 0)
@@ -433,10 +434,10 @@
     end(relay, 3, 0)()
     begin(3)
     end(relay, 3, 1)()
-    multiply(3, [middle(give_back, 1, 1)], True)
+    multiply(3, [end(give_back, 2, 0), middle(give_back, 1, 1)], True)
     cross(3, 0)
     cross(3, 1)
-    give_back(2, 0)
+    middle(give_back, 2, 0)()
     give_back(2, 1)
     middle(cross, 0, 0)()
     cross(0, 1)

time: 51.8 us -> 51.2 us (0.988)
  Pallas kernels: 50.9 us -> 50.3 us
    pallas_call x1, Pallas kernels: 50.9 us -> 50.3 us  [fused(): pl.pallas_call(functools.partial(fused_kernel, experts, groups, capacity)...]
where the time goes in v3:
time: 51.2 us; the launch traced here: 51 us
  Pallas kernels  50.3 us (98%)
  local copies, waits for them, and re-layouts  0.71 us (1%)
    pallas_call x1, Pallas kernels, fused(): pl.pallas_call(functools.partial(fused_kernel, experts, groups, capacity)...  50.3 us

profile of v3, /device:TPU:0, one launch (start us, length us, event | category | flops | bytes accessed | tf_op | source)
XLA Modules:
  0.0 51.0 jit_solution(16887203788309655296)
XLA Ops:
  0.0 50.3 %shard_map.82 = bf16[256,512]{1,0:T(8,128)(2,1)S(1)} custom-call(bf16[64,2048]{1,0:T(8,128)(2,1)} %tokens_hbm.1, f32[1,2048]{1,0:T(1,128)} %bitcast.4, s32[2,256]{1,0:T(2,128)} %bitcast.5, f32[2,256]{1,0:T(2,128)} %bitcast.6, bf16[1,2048,768]{2,1,0:T(8,128)(2,1)} %w_gate_hbm.1, bf16[1,2048,768]{2,1,0:T(8,128)(2,1)} %w_up_hbm.1, ...), custom_call_target="tpu_custom_call" | custom-call | tf_op jit(solution)/shard_map/pallas_call | solution.py:512
  50.3 0.7 %copy.10 = bf16[256,512]{1,0:T(8,128)(2,1)} copy(bf16[256,512]{1,0:T(8,128)(2,1)S(1)} %shard_map.82) | data formatting | bytes 524288
